TPU v7x, 32 devices: a whole 2x2x4 slice. The times are simulated.
32 devices in a mesh: ep: 4 (over y, x), tp: 8 (over z, core).
Axes of the slice: x: 2, y: 2, z: 4, core: 2. Of those that a mesh axis runs over, the one named last changes fastest.
Arguments:
- hidden: bfloat16 [64, 2048], P('ep'), may hold values from -6 to 6
- attn_gain: float32 [2048], replicated, may hold values from 0.1 to 1.9
- query_weight: bfloat16 [2048, 1024], P(None, 'tp'), may hold values from -0.125 to 0.125
- rotary_weight: bfloat16 [2048, 512], P(None, 'tp'), may hold values from -0.125 to 0.125
- key_up: bfloat16 [16, 64, 512], P('tp'), may hold values from -0.75 to 0.75
- cache_latent: bfloat16 [64, 4096, 512], P(('ep', 'tp'))
- cache_rotary: bfloat16 [64, 32, 4096], P(('ep', 'tp')), may hold values from -6 to 6
- lengths: int32 [64], P(('ep', 'tp')), may hold values from 1 to 4096, as said below
- value_up: bfloat16 [16, 512, 64], P('tp'), may hold values from -0.25 to 0.25
- out_weight: bfloat16 [1024, 2048], P('tp'), may hold values from -0.1875 to 0.1875
- mixed_gain: float32 [2048], replicated, may hold values from 0.1 to 1.9
- moe_gain: float32 [2048], replicated, may hold values from 0.1 to 1.9
- expert_ids: int32 [64, 2], replicated, may hold values from 0 to 3, all different within a row; in each aligned block of 16 rows (0 to 15, 16 to 31, ...) at most 16 rows name the same one
- route_logits: float32 [64, 2], replicated, may hold values from -6 to 6
- gate_weight: bfloat16 [4, 2048, 7168], P('ep', None, 'tp'), may hold values from -0.125 to 0.125
- up_weight: bfloat16 [4, 2048, 7168], P('ep', None, 'tp'), may hold values from -0.125 to 0.125
- down_weight: bfloat16 [4, 7168, 2048], P('ep', 'tp'), may hold values from -0.0625 to 0.0625
- final_gain: float32 [2048], replicated, may hold values from 0.1 to 1.9
Outputs:
- layer_out: bfloat16 [64, 2048], P(('ep', 'tp'))
Inputs may be any that keep to these rules, and one draw needn't show every extreme that they name: `lengths`: some sequence has exactly 4096 filled positions. `expert_ids`: within each aligned block of 16 rows no expert is named more than 16 times, a bound that some block reaches.
All inputs are finite; a program needn't handle non-finite values.
Results may differ from a plain program's by a relative error of at most 0.023.
The roundings to bfloat16 on the way count: a program that leaves them out, or rounds other values in their place, can miss the bound.
Values may be sent and summed in bfloat16 or wider, within the bound.
A program may use at most 64 MiB of HBM per device.

v0:
```python
import jax
import jax.numpy as jnp
from jax import lax
from jax.sharding import PartitionSpec as P

EPSILON = 1e-06


def norm_rows(values, gain_vector):
    values = values.astype(jnp.float32)
    factor = lax.rsqrt(jnp.mean(values * values, axis=-1, keepdims=True) + EPSILON)
    return values * factor * gain_vector


def rotate(values, position):
    half_width = values.shape[-1] // 2
    inverse = 10000.0 ** (-jnp.arange(half_width, dtype=jnp.float32) / half_width)
    angles = position.astype(jnp.float32)[:, None, None] * inverse
    cosine = jnp.cos(angles)
    sine_part = jnp.sin(angles)
    first_half = values[..., :half_width]
    second = values[..., half_width:]
    return jnp.concatenate(
        [first_half * cosine - second * sine_part, second * cosine + first_half * sine_part],
        axis=-1,
    )


def slot_tables(group_ids, group_probs, experts, capacity):
    row_count, top_count = group_ids.shape
    flat_ids = group_ids.reshape(-1)
    onehot = (flat_ids[:, None] == jnp.arange(experts, dtype=jnp.int32)[None, :]).astype(jnp.int32)
    earlier = jnp.cumsum(onehot, axis=0) - onehot
    slot_index = jnp.sum(earlier * onehot, axis=1)
    target = flat_ids * capacity + slot_index
    source = jnp.arange(row_count * top_count, dtype=jnp.int32) // top_count
    slot_rows = jnp.full((experts * capacity,), row_count, jnp.int32).at[target].set(source)
    slot_gates = (
        jnp.zeros((experts * capacity,), jnp.float32).at[target].set(group_probs.reshape(-1))
    )
    return (slot_rows, slot_gates)


def expert_rows(picked, gate_weight, up_weight, down_weight):
    gate_part = jnp.einsum("jnd,jdf->jnf", picked, gate_weight, preferred_element_type=jnp.float32)
    up_part = jnp.einsum("jnd,jdf->jnf", picked, up_weight, preferred_element_type=jnp.float32)
    act = (jax.nn.silu(gate_part) * up_part).astype(jnp.bfloat16)
    return jnp.einsum("jnf,jfd->jnd", act, down_weight, preferred_element_type=jnp.float32)


def body(
    hidden,
    attn_gain,
    query_weight,
    rotary_weight,
    key_up,
    cache_latent,
    cache_rotary,
    lengths,
    value_up,
    out_weight,
    mixed_gain,
    moe_gain,
    expert_ids,
    route_logits,
    gate_weight,
    up_weight,
    down_weight,
    final_gain,
):
    group_rows, features = hidden.shape
    local_heads, nope_width, latent_width = key_up.shape
    rotary_width = rotary_weight.shape[1] // local_heads
    own_rows = cache_latent.shape[0]
    groups = lax.axis_size("ep")
    own_start = lax.axis_index("tp") * own_rows
    normed_in = norm_rows(hidden, attn_gain).astype(jnp.bfloat16)
    query_nope = jnp.dot(normed_in, query_weight, preferred_element_type=jnp.float32).astype(
        jnp.bfloat16
    )
    query_nope = query_nope.reshape(group_rows, local_heads, nope_width)
    query_pe = jnp.dot(normed_in, rotary_weight, preferred_element_type=jnp.float32).astype(
        jnp.bfloat16
    )
    query_pe = query_pe.reshape(group_rows, local_heads, rotary_width)
    query_latent = jnp.einsum(
        "shn,hnc->shc", query_nope, key_up, preferred_element_type=jnp.float32
    ).astype(jnp.bfloat16)
    query_latent, query_pe = (
        lax.all_to_all(query_latent, "tp", split_axis=0, concat_axis=1, tiled=True),
        lax.all_to_all(query_pe, "tp", split_axis=0, concat_axis=1, tiled=True),
    )
    query_rot = rotate(query_pe.astype(jnp.float32), lengths - 1).astype(jnp.bfloat16)
    score_scale = (nope_width + rotary_width) ** (-0.5)
    scores = jnp.einsum(
        "bhc,bpc->bhp", query_latent, cache_latent, preferred_element_type=jnp.float32
    )
    scores = scores + jnp.einsum(
        "bhr,brp->bhp", query_rot, cache_rotary, preferred_element_type=jnp.float32
    )
    scores = scores * score_scale
    visible = (
        jnp.arange(cache_latent.shape[1], dtype=jnp.int32)[None, None, :] < lengths[:, None, None]
    )
    scores = jnp.where(visible, scores, -jnp.inf)
    highest = jnp.max(scores, axis=-1, keepdims=True)
    weights = jnp.exp(scores - highest)
    probs = (weights / jnp.sum(weights, axis=-1, keepdims=True)).astype(jnp.bfloat16)
    out_latent = jnp.einsum(
        "bhp,bpc->bhc", probs, cache_latent, preferred_element_type=jnp.float32
    ).astype(jnp.bfloat16)
    out_latent = lax.all_to_all(out_latent, "tp", split_axis=1, concat_axis=0, tiled=True)
    head_out = jnp.einsum(
        "shc,hcv->shv", out_latent, value_up, preferred_element_type=jnp.float32
    ).astype(jnp.bfloat16)
    head_terms = jnp.dot(
        head_out.reshape(group_rows, -1), out_weight, preferred_element_type=jnp.float32
    )
    attended = lax.psum(head_terms.astype(jnp.bfloat16), "tp")
    mixed_group = (hidden.astype(jnp.float32) + norm_rows(attended, mixed_gain)).astype(
        jnp.bfloat16
    )
    normed = norm_rows(mixed_group, moe_gain).astype(jnp.bfloat16)
    mixed_rows = lax.dynamic_slice_in_dim(mixed_group, own_start, own_rows, 0)
    local_experts = gate_weight.shape[0]
    experts_all = local_experts * groups
    top_count = expert_ids.shape[1]
    capacity = 2 * group_rows * top_count // experts_all
    gate_probs = jax.nn.softmax(route_logits, axis=-1)
    gathered = lax.all_gather(normed, "ep", axis=0, tiled=True)
    all_count = gathered.shape[0]

    def tables_for(group_ids, group_probs):
        return slot_tables(group_ids, group_probs, experts_all, capacity)

    slot_rows, slot_gates = jax.vmap(tables_for)(
        expert_ids.reshape(groups, group_rows, top_count),
        gate_probs.reshape(groups, group_rows, top_count),
    )
    offsets = jnp.arange(groups, dtype=jnp.int32)[:, None] * group_rows
    global_rows = jnp.where(slot_rows < group_rows, slot_rows + offsets, all_count)
    first_expert = lax.axis_index("ep") * local_experts
    my_rows = lax.dynamic_slice_in_dim(
        global_rows.reshape(groups, experts_all, capacity), first_expert, local_experts, 1
    )
    my_gates = lax.dynamic_slice_in_dim(
        slot_gates.reshape(groups, experts_all, capacity), first_expert, local_experts, 1
    )
    my_rows = my_rows.transpose(1, 0, 2).reshape(local_experts, groups * capacity)
    my_gates = my_gates.transpose(1, 0, 2).reshape(local_experts, groups * capacity)
    padded_all = jnp.concatenate([gathered, jnp.zeros((1, features), jnp.bfloat16)], axis=0)
    result = (
        expert_rows(padded_all[my_rows], gate_weight, up_weight, down_weight) * my_gates[..., None]
    )
    spread = (
        jnp.zeros((all_count + 1, features), jnp.float32)
        .at[my_rows.reshape(-1)]
        .add(result.reshape(-1, features))
    )
    routed = lax.psum_scatter(spread[:all_count], ("ep", "tp"), scatter_dimension=0, tiled=True)
    routed = routed.astype(jnp.bfloat16)
    return (mixed_rows.astype(jnp.float32) + norm_rows(routed, final_gain)).astype(jnp.bfloat16)


def solution(mesh):
    placed = (
        P("ep", None),
        P(),
        P(None, "tp"),
        P(None, "tp"),
        P("tp", None, None),
        P(("ep", "tp"), None, None),
        P(("ep", "tp"), None, None),
        P(("ep", "tp")),
        P("tp", None, None),
        P("tp", None),
        P(),
        P(),
        P(),
        P(),
        P("ep", None, "tp"),
        P("ep", None, "tp"),
        P("ep", "tp", None),
        P(),
    )
    return jax.shard_map(
        body, mesh=mesh, in_specs=placed, out_specs=P(("ep", "tp"), None), check_vma=False
    )
```

profile of v0, /device:TPU:0, one launch (start us, length us, event | category | flops | bytes accessed | tf_op | source)
XLA Modules:
  0.0 193.6 jit_solution(2101767761909809505)
XLA Ops:
  6.6 1.1 fusion.37
  7.6 1.2 convolution_convert_fusion.4
  8.9 0.7 reshape.273
  9.6 6.4 %all-to-all-start.1 = ((bf16[16,2,32]{2,1,0:T(2,128)(2,1)}), bf16[16,2,32]{2,1,0:T(2,128)(2,1)S(1)}, u32[]{:S(2)}, u32[]{:S(2)}) async-start(bf16[16,2,32]{2,1,0:T(2,128)(2,1)} %reshape.273), calls=%async_computation.1 | async-start | bytes 16384 | tf_op jit(solution)/shard_map/all_to_all | solution.py:91
  16.6 0.7 iota_compare_fusion.1
  17.3 0.8 copy.46
  19.7 6.4 %scatter_fusion = s32[4,64]{1,0:T(4,128)S(1)} fusion(s32[4,64]{1,0:T(4,128)S(1)} %broadcast.223, s32[128]{0:T(128)S(1)} %reshape.299, s32[128]{0:T(128)S(1)} %reshape.301), kind=kCustom, calls=%fused_computation.2 | custom fusion | bytes 2560 | tf_op jit(solution)/shard_map/vmap()/scatter | solution.py:37
  28.0 6.4 %scatter_fusion.1 = f32[4,64]{1,0:T(4,128)S(1)} fusion(f32[4,64]{1,0:T(4,128)S(1)} %broadcast_in_dim.26, s32[128]{0:T(128)S(1)} %reshape.299, f32[128]{0:T(128)S(1)} %reshape.307), kind=kCustom, calls=%fused_computation.3 | custom fusion | bytes 2560 | tf_op jit(solution)/shard_map/vmap()/scatter | solution.py:39
  34.5 5.1 %all-to-all-start = ((bf16[16,2,512]{2,1,0:T(2,128)(2,1)}), bf16[16,2,512]{2,1,0:T(2,128)(2,1)S(1)}, u32[]{:S(2)}, u32[]{:S(2)}) async-start(bf16[16,2,512]{2,1,0:T(2,128)(2,1)} %copy.39), calls=%async_computation | async-start | bytes 65536 | tf_op jit(solution)/shard_map/all_to_all | solution.py:90
  39.6 5.7 %all-to-all-done = bf16[16,2,512]{2,1,0:T(2,128)(2,1)S(1)} async-done(((bf16[16,2,512]{2,1,0:T(2,128)(2,1)}), bf16[16,2,512]{2,1,0:T(2,128)(2,1)S(1)}, u32[]{:S(2)}, u32[]{:S(2)}) %all-to-all-start) | async-done | bytes 32800 | tf_op jit(solution)/shard_map/all_to_all | solution.py:90
  45.3 5.7 %fusion.66 = f32[2,16,4096]{2,1,0:T(8,128)S(1)} fusion(bf16[2,16,512]{2,1,0:T(8,128)(2,1)S(1)} %all_to_all.36, bf16[2,4096,512]{2,1,0:T(8,128)(2,1)} %param.23), kind=kOutput, calls=%fused_computation.111 | convolution fusion | flops 134217728 | bytes 8945664 | tf_op jit(solution)/shard_map/bhc,bpc->bhp/dot_general | solution.py:95
  51.6 4.7 %convolution_convert_fusion.1 = bf16[2,16,512]{2,1,0:T(8,128)(2,1)S(1)} fusion(bf16[2,4096,512]{2,1,0:T(8,128)(2,1)} %param.23, f32[2,16]{1,0:T(2,128)S(1)} %fusion.65, f32[2,16,4096]{2,1,0:T(8,128)S(1)} %fusion.3), kind=kOutput, calls=%fused_computation.20 | convolution fusion | flops 134631456 | bytes 8945792 | tf_op jit(solution)/shard_map/bhp,bpc->bhc/dot_general | solution.py:109
  57.0 3.3 %all-to-all-start.2 = ((bf16[2,16,512]{2,0,1:T(2,128)(2,1)}), bf16[2,16,512]{2,0,1:T(2,128)(2,1)S(1)}, u32[]{:S(2)}, u32[]{:S(2)}) async-start(bf16[2,16,512]{2,0,1:T(2,128)(2,1)} %copy.42), calls=%async_computation.2 | async-start | bytes 65536 | tf_op jit(solution)/shard_map/all_to_all | solution.py:112
  60.4 5.6 %all-to-all-done.2 = bf16[2,16,512]{2,0,1:T(2,128)(2,1)S(1)} async-done(((bf16[2,16,512]{2,0,1:T(2,128)(2,1)}), bf16[2,16,512]{2,0,1:T(2,128)(2,1)S(1)}, u32[]{:S(2)}, u32[]{:S(2)}) %all-to-all-start.2) | async-done | bytes 32800 | tf_op jit(solution)/shard_map/all_to_all | solution.py:112
  66.3 0.8 convolution_convert_fusion
  67.3 53.0 %all-reduce.5.cloned.1.call-done = bf16[16,2048]{1,0:T(8,128)(2,1)} async-done(((bf16[16,2048]{1,0:T(8,128)(2,1)}), bf16[16,2048]{1,0:T(8,128)(2,1)}) %all-reduce.5.cloned.1.call-update) | async-done | bytes 65552 | tf_op jit(solution)/shard_map/psum | solution.py:119
  120.3 1.0 fusion.32
  121.3 1.1 fusion.34
  122.4 9.3 %all_gather.3 = bf16[64,2048]{1,0:T(8,128)(2,1)S(1)} all-gather(bf16[16,2048]{1,0:T(8,128)(2,1)S(1)} %fusion.36), channel_id=1, replica_groups=mesh['ep'=4,'tp'=8] {'ep'}, dimensions={0}, use_global_device_ids=true | all-gather | bytes 327680 | tf_op jit(solution)/shard_map/all_gather | solution.py:130
  131.7 0.7 gather_fusion
  132.5 2.7 %fusion.9 = f32[64,896]{1,0:T(8,128)S(1)} fusion(bf16[64,2048]{1,0:T(8,128)(2,1)S(1)} %gather_fusion, bf16[1,2048,896]{2,1,0:T(8,128)(2,1)} %param.32), kind=kOutput, calls=%fused_computation.14 | convolution fusion | flops 234881024 | bytes 4161536 | tf_op jit(solution)/shard_map/jnd,jdf->jnf/dot_general | solution.py:45
  135.2 4.7 %fusion.11 = f32[64,2048]{1,0:T(8,128)S(1)} fusion(bf16[1,896,2048]{2,1,0:T(8,128)(2,1)} %param.34, bf16[64,2048]{1,0:T(8,128)(2,1)S(1)} %gather_fusion, bf16[1,2048,896]{2,1,0:T(8,128)(2,1)} %param.33, f32[64]{0:T(128)S(1)} %mul.215, f32[64,896]{1,0:T(8,128)S(1)} %fusion.9), kind=kOutput, calls=%fused_computation.16 | convolution fusion | flops 470237184 | bytes 8356096 | tf_op jit(solution)/shard_map/jnf,jfd->jnd/dot_general | solution.py:48
  140.0 1.5 scatter_custom_fusion
  141.5 44.3 %all-reduce.6 = bf16[64,2048]{1,0:T(8,128)(2,1)S(1)} all-reduce(f32[64,2048]{1,0:T(8,128)S(1)} %slice.20), channel_id=2, replica_groups=mesh['ep'=4,'tp'=8] {'ep','tp'}, use_global_device_ids=true, to_apply=%region_13.14.clone | all-reduce | flops 131072 | bytes 786432
  (84 shorter events, 6.9 us)
Async XLA Ops:
  6.5 44.5 %copy-start = (bf16[2,32,4096]{2,1,0:T(8,128)(2,1)S(1)}, bf16[2,32,4096]{2,1,0:T(8,128)(2,1)}, u32[]{:S(2)}) copy-start(bf16[2,32,4096]{2,1,0:T(8,128)(2,1)} %param.24) | copy-start | bytes 1572868
  6.5 19.9 %copy-start.1 = (bf16[16,2048]{1,0:T(8,128)(2,1)S(1)}, bf16[16,2048]{1,0:T(8,128)(2,1)}, u32[]{:S(2)}) copy-start(bf16[16,2048]{1,0:T(8,128)(2,1)} %param.18) | copy-start | bytes 196612
  6.5 19.9 %copy-start.7 = (f32[2048]{0:T(1024)S(1)}, f32[2048]{0:T(1024)}, u32[]{:S(2)}) copy-start(f32[2048]{0:T(1024)} %param.19) | copy-start | bytes 24580
  6.5 19.9 %copy-start.3 = (bf16[2048,128]{1,0:T(8,128)(2,1)S(1)}, bf16[2048,128]{1,0:T(8,128)(2,1)}, u32[]{:S(2)}) copy-start(bf16[2048,128]{1,0:T(8,128)(2,1)} %param.20) | copy-start | bytes 1572868
  6.5 20.2 %copy-start.6 = (f32[64,2]{0,1:T(2,128)S(1)}, f32[64,2]{0,1:T(2,128)}, u32[]{:S(2)}) copy-start(f32[64,2]{0,1:T(2,128)} %param.31) | copy-start | bytes 1540
  6.5 20.4 %copy-start.4 = (bf16[2,64,512]{2,1,0:T(8,128)(2,1)S(1)}, bf16[2,64,512]{2,1,0:T(8,128)(2,1)}, u32[]{:S(2)}) copy-start(bf16[2,64,512]{2,1,0:T(8,128)(2,1)} %param.22) | copy-start | bytes 393220
  9.6 24.9 %all-to-all-start.1 = ((bf16[16,2,32]{2,1,0:T(2,128)(2,1)}), bf16[16,2,32]{2,1,0:T(2,128)(2,1)S(1)}, u32[]{:S(2)}, u32[]{:S(2)}) async-start(bf16[16,2,32]{2,1,0:T(2,128)(2,1)} %reshape.273), calls=%async_computation.1 | async-start | bytes 16384 | tf_op jit(solution)/shard_map/all_to_all | solution.py:91
  34.5 10.8 %all-to-all-start = ((bf16[16,2,512]{2,1,0:T(2,128)(2,1)}), bf16[16,2,512]{2,1,0:T(2,128)(2,1)S(1)}, u32[]{:S(2)}, u32[]{:S(2)}) async-start(bf16[16,2,512]{2,1,0:T(2,128)(2,1)} %copy.39), calls=%async_computation | async-start | bytes 65536 | tf_op jit(solution)/shard_map/all_to_all | solution.py:90
  51.6 14.5 %copy-start.5 = (bf16[2,512,64]{1,2,0:T(8,128)(2,1)S(1)}, bf16[2,512,64]{1,2,0:T(8,128)(2,1)}, u32[]{:S(2)}) copy-start(bf16[2,512,64]{1,2,0:T(8,128)(2,1)} %param.26) | copy-start | bytes 393220
  51.6 14.7 %copy-start.2 = (bf16[128,2048]{1,0:T(8,128)(2,1)S(1)}, bf16[128,2048]{1,0:T(8,128)(2,1)}, u32[]{:S(2)}) copy-start(bf16[128,2048]{1,0:T(8,128)(2,1)} %param.27) | copy-start | bytes 1572868
  51.6 69.7 %copy-start.8 = (f32[2048]{0:T(1024)S(1)}, f32[2048]{0:T(1024)}, u32[]{:S(2)}) copy-start(f32[2048]{0:T(1024)} %param.28) | copy-start | bytes 24580
  51.6 70.7 %copy-start.9 = (f32[2048]{0:T(1024)S(1)}, f32[2048]{0:T(1024)}, u32[]{:S(2)}) copy-start(f32[2048]{0:T(1024)} %param.29) | copy-start | bytes 24580
  57.0 9.0 %all-to-all-start.2 = ((bf16[2,16,512]{2,0,1:T(2,128)(2,1)}), bf16[2,16,512]{2,0,1:T(2,128)(2,1)S(1)}, u32[]{:S(2)}, u32[]{:S(2)}) async-start(bf16[2,16,512]{2,0,1:T(2,128)(2,1)} %copy.42), calls=%async_computation.2 | async-start | bytes 65536 | tf_op jit(solution)/shard_map/all_to_all | solution.py:112
  60.3 60.0 %all-reduce.5.cloned.1.call-start = ((), (), s32[]{:S(2)}) async-start(), calls=%async_computation.3 | async-start | bytes 131072 | tf_op jit(solution)/shard_map/psum | solution.py:119
  135.2 50.8 %copy-start.10 = (f32[2048]{0:T(1024)S(1)}, f32[2048]{0:T(1024)}, u32[]{:S(2)}) copy-start(f32[2048]{0:T(1024)} %param.35) | copy-start | bytes 24580
Sparse Core Ops, SparseCore 0:
  67.3 52.9 all-reduce.4
where the time goes:
time: 194 us
  waiting for transfers between devices  64.3 us (33%)
  blocking collectives  53.6 us (28%)
  matrix products  20.7 us (11%)
  local copies, waits for them, and re-layouts  17.8 us (9%)
  starting transfers between devices  14.8 us (8%)
  between operations  13.7 us (7%)
  other arithmetic  8.61 us (4%)
    psum x1, waiting for transfers between devices, body(): attended = lax.psum(head_terms.astype(jnp.bfloat16), 'tp')  53 us
    unnamed x1, blocking collectives  44.3 us
    all_gather x1, blocking collectives, body(): gathered = lax.all_gather(normed, 'ep', axis=0, tiled=True)  9.29 us
    scatter x2, local copies, waits for them, and re-layouts, slot_tables(): jnp.full((experts * capacity,), row_count, jnp.int32).at[target].set(source)  6.48 us
    scatter x1, local copies, waits for them, and re-layouts, slot_tables(): jnp.zeros((experts * capacity,), jnp.float32).at[target]  6.4 us
    all_to_all x1, starting transfers between devices, body(): lax.all_to_all(query_pe, 'tp', split_axis=0, concat_axis=1, tiled=True)  6.35 us
    dot_general x1, matrix products, body(): jnp.einsum('bhc,bpc->bhp', query_latent, cache_latent, preferred_element_...  5.66 us
    all_to_all x1, waiting for transfers between devices, body(): lax.all_to_all(query_latent, 'tp', split_axis=0, concat_axis=1, tiled=True)  5.65 us
  transfers between devices with their start and end apart: 4, of which 3 were waited for; matrix products, arithmetic and copies ran while one was open for 10% of the time, Pallas kernels for 0%

commit v1 on v0

v1 whole, which is shorter than its diff:
```python
import functools

import jax
import jax.numpy as jnp
import numpy as np
from jax import lax
from jax.experimental import pallas as pl
from jax.experimental.pallas import tpu as pltpu
from jax.sharding import PartitionSpec as P

EPSILON = 1e-06
F32 = jnp.float32
BF16 = jnp.bfloat16
MESH = pl.DeviceIdType.MESH


def rms(values, gain):
    factor = lax.rsqrt(jnp.mean(values * values, axis=-1, keepdims=True) + EPSILON)
    return values * factor * gain


def dot(a, b):
    return jnp.dot(a, b, preferred_element_type=F32)


def iota(shape, dim):
    return lax.broadcasted_iota(jnp.int32, shape, dim)


def kernel(
    dims,
    lengths,
    inverse,
    hidden_h,
    attn_gain_h,
    query_weight_h,
    rotary_weight_h,
    key_up_h,
    cache_rotary_h,
    cache_latent_h,
    value_up_h,
    out_weight_h,
    mixed_gain_h,
    moe_gain_h,
    expert_ids_h,
    logits_h,
    gate_weight_h,
    up_weight_h,
    down_weight_h,
    final_gain_h,
    out_ref,
    inverse_v,
    hidden,
    attn_gain,
    query_weight,
    rotary_weight,
    key_up,
    cache_rotary,
    cache_latent,
    value_up,
    out_weight,
    mixed_gain,
    moe_gain,
    expert_ids,
    logits,
    gate_weight,
    up_weight,
    down_weight,
    final_gain,
    q_stage,
    q_send,
    q_recv,
    q_rows,
    score_buf,
    o_stage,
    o_send,
    o_recv,
    o_rows,
    a_stage,
    a_send,
    a_recv,
    n_send,
    n_recv,
    x_stage,
    x_rows,
    act_buf,
    y_stage,
    y_send,
    y_recv,
    local_sem,
    send_sem,
    recv_sem,
):
    E, T, lh, nope, rope, own = dims
    N = E * T
    H = T * lh
    rows, features = hidden.shape
    latent = key_up.shape[1]
    cache_len = cache_latent.shape[1]
    all_rows = x_rows.shape[0]
    me_e = lax.axis_index("ep")
    me_t = lax.axis_index("tp")
    me = me_e * T + me_t

    pairs = [
        (hidden_h, hidden),
        (attn_gain_h, attn_gain),
        (query_weight_h, query_weight),
        (rotary_weight_h, rotary_weight),
        (key_up_h, key_up),
        (inverse, inverse_v),
        (cache_rotary_h, cache_rotary),
    ]
    cache_at = len(pairs)
    pairs += [(cache_latent_h.at[s], cache_latent.at[s]) for s in range(own)]
    rest_at = len(pairs)
    pairs += [
        (value_up_h, value_up),
        (out_weight_h, out_weight),
        (mixed_gain_h, mixed_gain),
        (moe_gain_h, moe_gain),
        (expert_ids_h, expert_ids),
        (logits_h, logits),
        (final_gain_h, final_gain),
    ]
    expert_at = len(pairs)
    pairs += [
        (gate_weight_h, gate_weight),
        (up_weight_h, up_weight),
        (down_weight_h, down_weight),
    ]
    copies = [
        pltpu.make_async_copy(src, dst, local_sem.at[i]) for i, (src, dst) in enumerate(pairs)
    ]
    for c in copies:
        c.start()

    barrier = pltpu.get_barrier_semaphore()

    def greet(i, carry):
        p = lax.rem(me + i, N)
        pl.semaphore_signal(
            barrier,
            inc=1,
            device_id={"ep": p // T, "tp": lax.rem(p, T)},
            device_id_type=MESH,
        )
        return carry

    lax.fori_loop(1, N, greet, 0)

    def tp_send(send, recv, k):
        def one(i, carry):
            p = lax.rem(me_t + i, T)
            pltpu.make_async_remote_copy(
                src_ref=send.at[p],
                dst_ref=recv.at[me_t],
                send_sem=send_sem.at[k],
                recv_sem=recv_sem.at[k],
                device_id={"tp": p},
                device_id_type=MESH,
            ).start()
            return carry

        lax.fori_loop(1, T, one, 0)

    def all_send(source, recv, k):
        def one(i, carry):
            p = lax.rem(me + i, N)
            pltpu.make_async_remote_copy(
                src_ref=source(p),
                dst_ref=recv.at[me],
                send_sem=send_sem.at[k],
                recv_sem=recv_sem.at[k],
                device_id={"ep": p // T, "tp": lax.rem(p, T)},
                device_id_type=MESH,
            ).start()
            return carry

        lax.fori_loop(1, N, one, 0)

    def await_bytes(buffer, sem, count):
        part = buffer.at[pl.ds(0, count)]
        pltpu.make_async_copy(part, part, sem).wait()

    for c in copies[:cache_at - 2]:
        c.wait()
    hid = hidden[...].astype(F32)
    normed_in = rms(hid, attn_gain[...]).astype(BF16)
    q_nope = dot(normed_in, query_weight[...]).astype(BF16)
    q_pe = dot(normed_in, rotary_weight[...]).astype(BF16)
    nope_head = iota(q_nope.shape, 1) // nope
    pe_head = iota(q_pe.shape, 1) // rope
    fold = (
        lax.rem(iota((lh * rope, rope), 0), rope) == iota((lh * rope, rope), 1)
    ).astype(BF16)
    q_stage[...] = jnp.zeros_like(q_stage)
    for h in range(lh):
        q_h = jnp.where(nope_head == h, q_nope, jnp.zeros_like(q_nope))
        q_stage[h, :, 0:latent] = dot(q_h, key_up[...])
        pe_h = jnp.where(pe_head == h, q_pe, jnp.zeros_like(q_pe))
        q_stage[h, :, latent:latent + rope] = dot(pe_h, fold)
    for j in range(T):
        for h in range(lh):
            q_send[j, h] = q_stage[h, own * j:own * (j + 1), :].astype(BF16)
    pl.semaphore_wait(barrier, N - 1)
    tp_send(q_send, q_recv, 0)
    q_recv[me_t] = q_send[me_t]

    inv = copies[cache_at - 2]
    inv.wait()
    copies[cache_at - 1].wait()
    await_bytes(q_recv, recv_sem.at[0], T - 1)
    for t in range(T):
        for h in range(lh):
            got = q_recv[t, h].astype(F32)
            at = t * lh + h
            for s in range(own):
                q_rows[s, at:at + 1, :] = got[s:s + 1, :]

    half = rope // 2
    turn_row = iota((rope, rope), 0)
    turn_col = iota((rope, rope), 1)
    turn = jnp.where(
        turn_row == turn_col + half,
        -1.0,
        jnp.where(turn_row == turn_col - half, 1.0, 0.0),
    ).astype(BF16)
    scale = (nope + rope) ** (-0.5)
    chunk = min(1024, cache_len)
    for s in range(own):
        length = lengths[s]
        angles = (length - 1).astype(F32) * inverse_v[...]
        pe = q_rows[s, :, latent:latent + rope]
        rot = (pe * jnp.cos(angles) + dot(pe.astype(BF16), turn) * jnp.sin(angles)).astype(BF16)
        lat = q_rows[s, :, 0:latent].astype(BF16)
        copies[cache_at + s].wait()
        for c in range(0, cache_len, chunk):
            part = lax.dot_general(
                lat,
                cache_latent[s, c:c + chunk, :],
                (((1,), (1,)), ((), ())),
                preferred_element_type=F32,
            )
            part = part + dot(rot, cache_rotary[s, :, c:c + chunk])
            seen = iota(part.shape, 1) + c < length
            score_buf[:, c:c + chunk] = jnp.where(seen, part * scale, -jnp.inf)
        highest = jnp.max(score_buf[...], axis=-1, keepdims=True)
        weights = jnp.exp(score_buf[...] - highest)
        total = jnp.sum(weights, axis=-1, keepdims=True)
        probs = (weights / total).astype(BF16)
        acc = jnp.zeros((H, latent), F32)
        for c in range(0, cache_len, chunk):
            acc = acc + dot(probs[:, c:c + chunk], cache_latent[s, c:c + chunk, :])
        o_stage[s] = acc
    for t in range(T):
        for s in range(own):
            o_send[t, s] = o_stage[s, t * lh:(t + 1) * lh, :].astype(BF16)
    tp_send(o_send, o_recv, 1)
    o_recv[me_t] = o_send[me_t]
    for c in copies[rest_at:expert_at]:
        c.wait()
    gate_probs = jax.nn.softmax(logits[...], axis=-1)
    row_gates = jnp.sum(
        jnp.where(expert_ids[...] == me_e, gate_probs, 0.0), axis=-1, keepdims=True
    )
    pick = (iota((own, rows), 1) == iota((own, rows), 0) + me_t * own).astype(BF16)
    hidden_own = dot(pick, hidden[...])

    await_bytes(o_recv, recv_sem.at[1], T - 1)
    for j in range(T):
        for s in range(own):
            got = o_recv[j, s].astype(F32)
            at = j * own + s
            for h in range(lh):
                o_rows[h, at:at + 1, :] = got[h:h + 1, :]
    terms = jnp.zeros((rows, features), F32)
    for h in range(lh):
        o_h = o_rows[h].astype(BF16)
        head_out = dot(o_h, value_up[h]).astype(BF16)
        width = head_out.shape[1]
        terms = terms + dot(head_out, out_weight[h * width:(h + 1) * width, :])
    a_stage[...] = terms
    for j in range(T):
        a_send[j] = a_stage[own * j:own * (j + 1), :].astype(BF16)
    tp_send(a_send, a_recv, 2)
    a_recv[me_t] = a_send[me_t]
    await_bytes(a_recv, recv_sem.at[2], T - 1)
    attended = jnp.zeros((own, features), F32)
    for j in range(T):
        attended = attended + a_recv[j].astype(F32)
    attended = attended.astype(BF16).astype(F32)
    mixed = (hidden_own + rms(attended, mixed_gain[...])).astype(BF16).astype(F32)
    n_send[0] = rms(mixed, moe_gain[...]).astype(BF16)

    all_send(lambda p: n_send.at[0], n_recv, 3)
    n_recv[me] = n_send[0]
    for c in copies[expert_at:]:
        c.wait()
    await_bytes(n_recv, recv_sem.at[3], N - 1)
    for j in range(N):
        x_stage[own * j:own * (j + 1), :] = n_recv[j].astype(F32)
    x_rows[...] = x_stage[...].astype(BF16)
    block = min(64, all_rows)
    step = min(512, features)

    def run_block(b, carry):
        at = pl.ds(pl.multiple_of(b * block, block), block)
        picked = x_rows[at, :]
        gate_part = dot(picked, gate_weight[0])
        up_part = dot(picked, up_weight[0])
        act_buf[at, :] = (gate_part / (1.0 + jnp.exp(-gate_part)) * up_part).astype(BF16)
        for c in range(0, features, step):
            y_stage[at, c:c + step] = dot(act_buf[at, :], down_weight[0, :, c:c + step])
        return carry

    if block == all_rows:
        run_block(0, 0)
    else:
        lax.fori_loop(0, all_rows // block, run_block, 0)
    y_stage[...] = y_stage[...] * row_gates
    for j in range(N):
        y_send[j] = y_stage[own * j:own * (j + 1), :].astype(BF16)
    all_send(lambda p: y_send.at[p], y_recv, 4)
    y_recv[me] = y_send[me]
    await_bytes(y_recv, recv_sem.at[4], N - 1)

    def add(j, acc):
        return acc + y_recv[j].astype(F32)

    routed = lax.fori_loop(0, N, add, jnp.zeros((own, features), F32), unroll=8)
    routed = routed.astype(BF16).astype(F32)
    out_ref[...] = (mixed + rms(routed, final_gain[...])).astype(BF16)

    await_bytes(q_send, send_sem.at[0], T - 1)
    await_bytes(o_send, send_sem.at[1], T - 1)
    await_bytes(a_send, send_sem.at[2], T - 1)
    await_bytes(n_recv, send_sem.at[3], N - 1)
    await_bytes(y_send, send_sem.at[4], N - 1)


def body(
    hidden,
    attn_gain,
    query_weight,
    rotary_weight,
    key_up,
    cache_latent,
    cache_rotary,
    lengths,
    value_up,
    out_weight,
    mixed_gain,
    moe_gain,
    expert_ids,
    route_logits,
    gate_weight,
    up_weight,
    down_weight,
    final_gain,
):
    E, T = lax.axis_size("ep"), lax.axis_size("tp")
    N = E * T
    rows, features = hidden.shape
    lh, nope, latent = key_up.shape
    rope = rotary_weight.shape[1] // lh
    own, cache_len, _ = cache_latent.shape
    H = T * lh
    all_rows = expert_ids.shape[0]
    ff = gate_weight.shape[2]
    wide = latent + 128
    freq = (10000.0 ** (-np.arange(rope // 2, dtype=np.float32) / (rope // 2))).astype(np.float32)
    inverse = jnp.asarray(np.concatenate([freq, freq])[None, :])
    arrays = [
        inverse,
        hidden,
        attn_gain.reshape(1, -1),
        query_weight,
        rotary_weight,
        key_up.reshape(lh * nope, latent),
        cache_rotary,
        cache_latent,
        value_up,
        out_weight,
        mixed_gain.reshape(1, -1),
        moe_gain.reshape(1, -1),
        expert_ids,
        route_logits,
        gate_weight,
        up_weight,
        down_weight,
        final_gain.reshape(1, -1),
    ]
    anywhere = pl.BlockSpec(memory_space=pl.ANY)
    v = pltpu.VMEM
    n_copies = len(arrays) - 1 + own
    scratch = [v(a.shape, a.dtype) for a in arrays] + [
        v((lh, rows, wide), F32),
        v((T, lh, own, wide), BF16),
        v((T, lh, own, wide), BF16),
        v((own, H, wide), F32),
        v((H, cache_len), F32),
        v((own, H, latent), F32),
        v((T, own, lh, latent), BF16),
        v((T, own, lh, latent), BF16),
        v((lh, rows, latent), F32),
        v((rows, features), F32),
        v((T, own, features), BF16),
        v((T, own, features), BF16),
        v((1, own, features), BF16),
        v((N, own, features), BF16),
        v((all_rows, features), F32),
        v((all_rows, features), BF16),
        v((all_rows, ff), BF16),
        v((all_rows, features), F32),
        v((N, own, features), BF16),
        v((N, own, features), BF16),
        pltpu.SemaphoreType.DMA((n_copies,)),
        pltpu.SemaphoreType.DMA((5,)),
        pltpu.SemaphoreType.DMA((5,)),
    ]
    return pl.pallas_call(
        functools.partial(kernel, (E, T, lh, nope, rope, own)),
        out_shape=jax.ShapeDtypeStruct((own, features), BF16),
        in_specs=[pl.BlockSpec(memory_space=pltpu.SMEM)] + [anywhere] * len(arrays),
        out_specs=pl.BlockSpec(memory_space=pltpu.VMEM),
        scratch_shapes=scratch,
        compiler_params=pltpu.CompilerParams(
            collective_id=0,
            has_side_effects=True,
            vmem_limit_bytes=62 * 1024 * 1024,
        ),
    )(lengths, *arrays)


def solution(mesh):
    placed = (
        P("ep", None),
        P(),
        P(None, "tp"),
        P(None, "tp"),
        P("tp", None, None),
        P(("ep", "tp"), None, None),
        P(("ep", "tp"), None, None),
        P(("ep", "tp")),
        P("tp", None, None),
        P("tp", None),
        P(),
        P(),
        P(),
        P(),
        P("ep", None, "tp"),
        P("ep", None, "tp"),
        P("ep", "tp", None),
        P(),
    )
    return jax.shard_map(
        body, mesh=mesh, in_specs=placed, out_specs=P(("ep", "tp"), None), check_vma=False
    )
```

time: 194 us -> 49.4 us (0.25)
  waiting for transfers between devices: 64.3 us -> 0 us
  blocking collectives: 53.6 us -> 0 us
  Pallas kernels: 0 us -> 41.4 us
  matrix products: 20.7 us -> 0 us
  starting transfers between devices: 14.8 us -> 0 us
  between operations: 13.7 us -> 0.01 us
  local copies, waits for them, and re-layouts: 17.8 us -> 7.72 us
  other arithmetic: 8.61 us -> 0 us
    psum x1 -> x0, waiting for transfers between devices: 53 us -> none  [body(): attended = lax.psum(head_terms.astype(jnp.bfloat16), 'tp')]
    unnamed x1 -> x0, blocking collectives: 44.3 us -> none
    pallas_call x0 -> x1, Pallas kernels: none -> 41.4 us  [body(): pl.pallas_call(functools.partial(kernel, (E, T, lh, nope, rope, own)), ou...]
    dot_general x10 -> x0, matrix products: 20.7 us -> none  [the longest x1 5.66 us: body(): jnp.einsum('bhc,bpc->bhp', query_latent, cache_latent, preferred_element_...]
    all_to_all x3 -> x0, starting transfers between devices: 14.8 us -> none  [the longest x1 6.35 us: body(): lax.all_to_all(query_pe, 'tp', split_axis=0, concat_axis=1, tiled=True)]
    scatter x3 -> x0, local copies, waits for them, and re-layouts: 12.9 us -> none  [the longest x2 6.48 us: slot_tables(): jnp.full((experts * capacity,), row_count, jnp.int32).at[target].set(source)]
    all_to_all x3 -> x0, waiting for transfers between devices: 11.3 us -> none  [the longest x1 5.65 us: body(): lax.all_to_all(query_latent, 'tp', split_axis=0, concat_axis=1, tiled=True)]
    all_gather x1 -> x0, blocking collectives: 9.29 us -> none  [body(): gathered = lax.all_gather(normed, 'ep', axis=0, tiled=True)]
  transfers between devices with their start and end apart: 4 -> 0, of which waited for: 3 -> 0; matrix products, arithmetic and copies ran while one was open for 10% -> 0% of each run, Pallas kernels for 0% -> 0%
where the time goes in v1:
time: 49.4 us; the launch traced here: 49.1 us
  Pallas kernels  41.4 us (84%)
  local copies, waits for them, and re-layouts  7.72 us (16%)
    pallas_call x1, Pallas kernels, body(): pl.pallas_call(functools.partial(kernel, (E, T, lh, nope, rope, own)), ou...  41.4 us
    unnamed x5, local copies, waits for them, and re-layouts  7.72 us

profile of v1, /device:TPU:0, one launch (start us, length us, event | category | flops | bytes accessed | tf_op | source)
XLA Modules:
  0.0 49.1 jit_solution(7917594796168628969)
XLA Ops:
  0.0 1.4 %copy.22.expert_ids_h = s32[64,2]{1,0:T(8,128)} copy(s32[64,2]{0,1:T(2,128)} %param.31) | data formatting | bytes 1024 | tf_op args[12]
  1.4 1.4 %copy.23.logits_h = f32[64,2]{1,0:T(8,128)} copy(f32[64,2]{0,1:T(2,128)} %param.32) | data formatting | bytes 1024 | tf_op args[13]
  2.7 1.7 %copy.21.value_up_h = bf16[2,512,64]{2,1,0:T(8,128)(2,1)} copy(bf16[2,512,64]{1,2,0:T(8,128)(2,1)} %param.27) | data formatting | bytes 262144 | tf_op args[8]
  4.5 1.9 %copy.20.rotary_weight_h = bf16[2048,64]{1,0:T(8,128)(2,1)} copy(bf16[2048,64]{0,1:T(8,128)(2,1)} %param.22) | data formatting | bytes 524288 | tf_op args[3]
  6.4 41.4 %shard_map.181 = bf16[2,2048]{1,0:T(2,128)(2,1)} custom-call(s32[2]{0:T(128)} %lengths.1, f32[1,32]{1,0:T(1,128)} %constant.2.clone.inverse, bf16[16,2048]{1,0:T(8,128)(2,1)} %hidden_h.1, f32[1,2048]{1,0:T(1,128)} %bitcast.6, bf16[2048,128]{1,0:T(8,128)(2,1)} %query_weight_h.1, bf16[2048,64]{1,0:T(8,128)(2,1)} %copy.20.rotary_weight_h, ...), custom_call_target="tpu_custom_call" | custom-call | tf_op jit(solution)/shard_map/pallas_call | solution.py:422
  47.8 1.3 %copy.25 = bf16[2,2048]{1,0:T(2,128)(2,1)} copy(bf16[2,2048]{1,0:T(2,128)(2,1)} %shard_map.181) | data formatting | bytes 16384

commit v2 on v1

--- a/solution.py
+++ b/solution.py
@@ -21,6 +21,10 @@
 
 def dot(a, b):
     return jnp.dot(a, b, preferred_element_type=F32)
+
+
+def dot_t(a, b):
+    return lax.dot_general(a, b, (((1,), (1,)), ((), ())), preferred_element_type=F32)
 
 
 def iota(shape, dim):
@@ -81,7 +85,6 @@
     a_recv,
     n_send,
     n_recv,
-    x_stage,
     x_rows,
     act_buf,
     y_stage,
@@ -90,6 +93,7 @@
     local_sem,
     send_sem,
     recv_sem,
+    chip_sem,
 ):
     E, T, lh, nope, rope, own = dims
     N = E * T
@@ -188,7 +192,7 @@
     hid = hidden[...].astype(F32)
     normed_in = rms(hid, attn_gain[...]).astype(BF16)
     q_nope = dot(normed_in, query_weight[...]).astype(BF16)
-    q_pe = dot(normed_in, rotary_weight[...]).astype(BF16)
+    q_pe = dot_t(normed_in, rotary_weight[...]).astype(BF16)
     nope_head = iota(q_nope.shape, 1) // nope
     pe_head = iota(q_pe.shape, 1) // rope
     fold = (
@@ -236,12 +240,7 @@
         lat = q_rows[s, :, 0:latent].astype(BF16)
         copies[cache_at + s].wait()
         for c in range(0, cache_len, chunk):
-            part = lax.dot_general(
-                lat,
-                cache_latent[s, c:c + chunk, :],
-                (((1,), (1,)), ((), ())),
-                preferred_element_type=F32,
-            )
+            part = dot_t(lat, cache_latent[s, c:c + chunk, :])
             part = part + dot(rot, cache_rotary[s, :, c:c + chunk])
             seen = iota(part.shape, 1) + c < length
             score_buf[:, c:c + chunk] = jnp.where(seen, part * scale, -jnp.inf)
@@ -260,9 +259,13 @@
     o_recv[me_t] = o_send[me_t]
     for c in copies[rest_at:expert_at]:
         c.wait()
-    gate_probs = jax.nn.softmax(logits[...], axis=-1)
+    gate_probs = jax.nn.softmax(logits[...], axis=0)
+    gate_line = jnp.sum(
+        jnp.where(expert_ids[...] == me_e, gate_probs, 0.0), axis=0, keepdims=True
+    )
+    square = (all_rows, all_rows)
     row_gates = jnp.sum(
-        jnp.where(expert_ids[...] == me_e, gate_probs, 0.0), axis=-1, keepdims=True
+        jnp.where(iota(square, 0) == iota(square, 1), gate_line, 0.0), axis=-1, keepdims=True
     )
     pick = (iota((own, rows), 1) == iota((own, rows), 0) + me_t * own).astype(BF16)
     hidden_own = dot(pick, hidden[...])
@@ -277,7 +280,7 @@
     terms = jnp.zeros((rows, features), F32)
     for h in range(lh):
         o_h = o_rows[h].astype(BF16)
-        head_out = dot(o_h, value_up[h]).astype(BF16)
+        head_out = dot_t(o_h, value_up[h]).astype(BF16)
         width = head_out.shape[1]
         terms = terms + dot(head_out, out_weight[h * width:(h + 1) * width, :])
     a_stage[...] = terms
@@ -293,14 +296,45 @@
     mixed = (hidden_own + rms(attended, mixed_gain[...])).astype(BF16).astype(F32)
     n_send[0] = rms(mixed, moe_gain[...]).astype(BF16)
 
-    all_send(lambda p: n_send.at[0], n_recv, 3)
+    side = lax.rem(me, 2)
+    chips = N // 2
+
+    def place(p):
+        return {"ep": p // T, "tp": lax.rem(p, T)}
+
+    def spread(source, slot, target, sem):
+        pltpu.make_async_remote_copy(
+            src_ref=source,
+            dst_ref=n_recv.at[slot],
+            send_sem=send_sem.at[3],
+            recv_sem=sem,
+            device_id=place(target),
+            device_id_type=MESH,
+        ).start()
+
+    pair = me + 1 - 2 * side
+
+    def outward(i, carry):
+        spread(n_send.at[0], me, 2 * lax.rem(me // 2 + i, chips) + side, chip_sem.at[me // 2])
+        return carry
+
+    lax.fori_loop(1, chips, outward, 0)
+    spread(n_send.at[0], me, pair, recv_sem.at[3])
     n_recv[me] = n_send[0]
+
+    def hand_on(i, carry):
+        chip = lax.rem(me // 2 + chips - i, chips)
+        p = 2 * chip + side
+        pltpu.make_async_copy(n_recv.at[p], n_recv.at[p], chip_sem.at[chip]).wait()
+        spread(n_recv.at[p], p, pair, recv_sem.at[3])
+        return carry
+
+    lax.fori_loop(1, chips, hand_on, 0)
     for c in copies[expert_at:]:
         c.wait()
-    await_bytes(n_recv, recv_sem.at[3], N - 1)
+    await_bytes(n_recv, recv_sem.at[3], chips)
     for j in range(N):
-        x_stage[own * j:own * (j + 1), :] = n_recv[j].astype(F32)
-    x_rows[...] = x_stage[...].astype(BF16)
+        x_rows[own * j:own * (j + 1), :] = n_recv[j]
     block = min(64, all_rows)
     step = min(512, features)
 
@@ -376,16 +410,16 @@
         hidden,
         attn_gain.reshape(1, -1),
         query_weight,
-        rotary_weight,
+        rotary_weight.T,
         key_up.reshape(lh * nope, latent),
         cache_rotary,
         cache_latent,
-        value_up,
+        value_up.transpose(0, 2, 1),
         out_weight,
         mixed_gain.reshape(1, -1),
         moe_gain.reshape(1, -1),
-        expert_ids,
-        route_logits,
+        expert_ids.T,
+        route_logits.T,
         gate_weight,
         up_weight,
         down_weight,
@@ -409,7 +443,6 @@
         v((T, own, features), BF16),
         v((1, own, features), BF16),
         v((N, own, features), BF16),
-        v((all_rows, features), F32),
         v((all_rows, features), BF16),
         v((all_rows, ff), BF16),
         v((all_rows, features), F32),
@@ -418,6 +451,7 @@
         pltpu.SemaphoreType.DMA((n_copies,)),
         pltpu.SemaphoreType.DMA((5,)),
         pltpu.SemaphoreType.DMA((5,)),
+        pltpu.SemaphoreType.DMA((N // 2,)),
     ]
     return pl.pallas_call(
         functools.partial(kernel, (E, T, lh, nope, rope, own)),

time: 49.4 us -> 41.7 us (0.84)
  local copies, waits for them, and re-layouts: 7.72 us -> 1.3 us
  Pallas kernels: 41.4 us -> 40.1 us
    unnamed x5 -> x1, local copies, waits for them, and re-layouts: 7.72 us -> 1.3 us
    pallas_call x1, Pallas kernels: 41.4 us -> 40.1 us  [body(): pl.pallas_call(functools.partial(kernel, (E, T, lh, nope, rope, own)), ou...]
where the time goes in v2:
time: 41.7 us; the launch traced here: 41.5 us
  Pallas kernels  40.1 us (96%)
  local copies, waits for them, and re-layouts  1.3 us (3%)
    pallas_call x1, Pallas kernels, body(): pl.pallas_call(functools.partial(kernel, (E, T, lh, nope, rope, own)), ou...  40.1 us
    unnamed x1, local copies, waits for them, and re-layouts  1.3 us

profile of v2, /device:TPU:0, one launch (start us, length us, event | category | flops | bytes accessed | tf_op | source)
XLA Modules:
  0.0 41.5 jit_solution(3334392731445227434)
XLA Ops:
  0.0 40.1 %shard_map.181 = bf16[2,2048]{1,0:T(2,128)(2,1)} custom-call(s32[2]{0:T(128)} %lengths.1, f32[1,32]{1,0:T(1,128)} %constant.2.clone.inverse, bf16[16,2048]{1,0:T(8,128)(2,1)} %hidden_h.1, f32[1,2048]{1,0:T(1,128)} %bitcast.12, bf16[2048,128]{1,0:T(8,128)(2,1)} %query_weight_h.1, bf16[64,2048]{1,0:T(8,128)(2,1)} %bitcast.9, bf16[128,512]{1,0:T(8,128)(2,1)} %bitcast.10, ...), custom_call_target="tpu_custom_call" | custom-call | tf_op jit(solution)/shard_map/pallas_call | solution.py:456
  40.1 1.3 %copy.21 = bf16[2,2048]{1,0:T(2,128)(2,1)} copy(bf16[2,2048]{1,0:T(2,128)(2,1)} %shard_map.181) | data formatting | bytes 16384
